TPU v7x, 32 devices: a whole 2x2x4 slice. The times are simulated.
32 devices in a mesh: kv: 4 (over y, x), tp: 8 (over z, core).
Axes of the slice: x: 2, y: 2, z: 4, core: 2. Of those that a mesh axis runs over, the one named last changes fastest.
Arguments:
- tokens: bfloat16 [256, 4096], P(None, ('kv', 'tp')), may hold values from -10 to 10
- past_state: float32 [256, 32, 64, 128], P('kv', 'tp'), may hold values from -6 to 6
- first_gain: float32 [4096], P('kv'), may hold values from 0.1 to 1.9
- first_gate: bfloat16 [4096, 11264], P('kv', 'tp'), may hold values from -0.09375 to 0.09375
- first_up: bfloat16 [4096, 11264], P('kv', 'tp'), may hold values from -0.09375 to 0.09375
- first_down: bfloat16 [11264, 4096], P('tp', 'kv'), may hold values from -0.078125 to 0.078125
- mix_gain: float32 [4096], P('kv'), may hold values from 0.1 to 1.9
- query_weight: bfloat16 [4096, 2048], P('kv', 'tp'), may hold values from -0.09375 to 0.09375
- key_weight: bfloat16 [4096, 2048], P('kv', 'tp'), may hold values from -0.09375 to 0.09375
- value_weight: bfloat16 [4096, 4096], P('kv', 'tp'), may hold values from -0.09375 to 0.09375
- output_gate_weight: bfloat16 [4096, 4096], P('kv', 'tp'), may hold values from -0.09375 to 0.09375
- head_gain: float32 [4096], P('tp'), may hold values from 0.1 to 1.9
- out_weight: bfloat16 [4096, 4096], P('tp', 'kv'), may hold values from -0.125 to 0.125
- second_gain: float32 [4096], P('kv'), may hold values from 0.1 to 1.9
- second_gate: bfloat16 [4096, 11264], P('kv', 'tp'), may hold values from -0.09375 to 0.09375
- second_up: bfloat16 [4096, 11264], P('kv', 'tp'), may hold values from -0.09375 to 0.09375
- second_down: bfloat16 [11264, 4096], P('tp', 'kv'), may hold values from -0.078125 to 0.078125
Outputs:
- mixed: bfloat16 [256, 4096], P(None, ('kv', 'tp'))
- new_state: float32 [256, 32, 64, 128], P('kv', 'tp')
All inputs are finite; a program needn't handle non-finite values.
Results may differ from a plain program's by a relative error of at most 0.033.
Values may be sent and summed in bfloat16 or wider, within the bound.
A program may use at most 128 MiB of HBM per device.

v0:
```python
import jax
import jax.numpy as jnp
from jax import lax
from jax.sharding import PartitionSpec as P

D = 4096
HEADS = 32
HEAD_K = 64
HEAD_V = 128
POS = 16384
EPS_RMS = 1e-06
EPS_GROUP = 1e-05
ROPE_BASE = 10000.0


def rotate(vectors):
    half_width = vectors.shape[-1] // 2
    frequency = ROPE_BASE ** (-jnp.arange(half_width, dtype=jnp.float32) / half_width)
    angles = POS * frequency
    cosine = jnp.cos(angles)
    sine_part = jnp.sin(angles)
    lower = vectors[..., :half_width]
    upper = vectors[..., half_width:]
    return jnp.concatenate(
        [lower * cosine - upper * sine_part, lower * sine_part + upper * cosine], axis=-1
    )


def activate(gate_sum, up_sum, summed):
    inverse_rms = lax.rsqrt(summed / D + EPS_RMS)[:, None]
    return (jax.nn.silu(gate_sum * inverse_rms) * (up_sum * inverse_rms)).astype(jnp.bfloat16)


def channel_mix(widened, gain, w_gate, w_up, w_down):
    widened_f = widened.astype(jnp.float32)
    scaled = (widened_f * gain).astype(jnp.bfloat16)
    squares = jnp.sum(widened_f * widened_f, axis=1)
    gate_part = jnp.dot(scaled, w_gate, preferred_element_type=jnp.float32)
    up_part = jnp.dot(scaled, w_up, preferred_element_type=jnp.float32)
    gate_sum, up_sum, summed = (
        lax.psum(gate_part.astype(jnp.bfloat16), "kv").astype(jnp.float32),
        lax.psum(up_part.astype(jnp.bfloat16), "kv").astype(jnp.float32),
        lax.psum(squares.astype(jnp.bfloat16), "kv").astype(jnp.float32),
    )
    return 0.5 * jnp.dot(
        activate(gate_sum, up_sum, summed), w_down, preferred_element_type=jnp.float32
    )


def token_mix(
    widened,
    past_state,
    gain,
    query_weight,
    key_weight,
    value_weight,
    output_gate_weight,
    head_gain,
    out_weight,
):
    widened_f = widened.astype(jnp.float32)
    scaled = (widened_f * gain).astype(jnp.bfloat16)
    squares = jnp.sum(widened_f * widened_f, axis=1)
    query_part = jnp.dot(scaled, query_weight, preferred_element_type=jnp.float32)
    key_part = jnp.dot(scaled, key_weight, preferred_element_type=jnp.float32)
    value_part = jnp.dot(scaled, value_weight, preferred_element_type=jnp.float32)
    gate_part = jnp.dot(scaled, output_gate_weight, preferred_element_type=jnp.float32)
    queries, keys_now, values_now, gate_now, summed = (
        lax.psum_scatter(
            query_part.astype(jnp.bfloat16), "kv", scatter_dimension=0, tiled=True
        ).astype(jnp.float32),
        lax.psum_scatter(
            key_part.astype(jnp.bfloat16), "kv", scatter_dimension=0, tiled=True
        ).astype(jnp.float32),
        lax.psum_scatter(
            value_part.astype(jnp.bfloat16), "kv", scatter_dimension=0, tiled=True
        ).astype(jnp.float32),
        lax.psum_scatter(
            gate_part.astype(jnp.bfloat16), "kv", scatter_dimension=0, tiled=True
        ).astype(jnp.float32),
        lax.psum_scatter(
            squares.astype(jnp.bfloat16), "kv", scatter_dimension=0, tiled=True
        ).astype(jnp.float32),
    )
    inverse_rms = lax.rsqrt(summed / D + EPS_RMS)[:, None]
    row_count = past_state.shape[0]
    local_heads = past_state.shape[1]
    queries = rotate((queries * inverse_rms).reshape(row_count, local_heads, HEAD_K)) * HEAD_K ** (
        -0.5
    )
    keys_now = rotate((keys_now * inverse_rms).reshape(row_count, local_heads, HEAD_K))
    values_now = (values_now * inverse_rms).reshape(row_count, local_heads, HEAD_V)
    gate_now = gate_now * inverse_rms
    head_level = (lax.axis_index("tp") * local_heads + jnp.arange(local_heads)).astype(jnp.float32)
    retained = 1.0 - jnp.exp2(-5.0 - 16.0 * head_level / (HEADS - 1))
    new_state = (
        retained[None, :, None, None] * past_state
        + keys_now[:, :, :, None] * values_now[:, :, None, :]
    )
    retrieved = jnp.einsum("bhk,bhkv->bhv", queries, new_state, precision=lax.Precision.HIGHEST)
    head_mean = jnp.mean(retrieved, axis=-1, keepdims=True)
    variance = jnp.mean(jnp.square(retrieved - head_mean), axis=-1, keepdims=True)
    normed = ((retrieved - head_mean) * lax.rsqrt(variance + EPS_GROUP)).reshape(
        row_count, local_heads * HEAD_V
    )
    mixed_heads = (jax.nn.silu(gate_now) * (normed * head_gain)).astype(jnp.bfloat16)
    projected = jnp.dot(
        lax.all_gather(mixed_heads, "kv", axis=0, tiled=True),
        out_weight,
        preferred_element_type=jnp.float32,
    )
    return (projected, new_state)


def shards(
    tokens,
    past_state,
    first_gain,
    first_gate,
    first_up,
    first_down,
    mix_gain,
    query_weight,
    key_weight,
    value_weight,
    output_gate_weight,
    head_gain,
    out_weight,
    second_gain,
    second_gate,
    second_up,
    second_down,
):

    def first_section(widened):
        return (channel_mix(widened, first_gain, first_gate, first_up, first_down), None)

    def middle_section(widened):
        return token_mix(
            widened,
            past_state,
            mix_gain,
            query_weight,
            key_weight,
            value_weight,
            output_gate_weight,
            head_gain,
            out_weight,
        )

    def last_section(widened):
        return (channel_mix(widened, second_gain, second_gate, second_up, second_down), None)

    sections = [first_section, middle_section, last_section]
    own_columns = tokens
    widened = lax.all_gather(tokens, "tp", axis=1, tiled=True)
    state_out = past_state
    for section_index in range(3):
        branch_out, produced = sections[section_index](widened)
        if produced is not None:
            state_out = produced
        own_piece = lax.psum_scatter(
            branch_out.astype(jnp.bfloat16), "tp", scatter_dimension=1, tiled=True
        ).astype(jnp.float32)
        own_columns = (own_columns.astype(jnp.float32) + own_piece).astype(jnp.bfloat16)
        if section_index < 2:
            widened = lax.all_gather(own_columns, "tp", axis=1, tiled=True)
    return (own_columns, state_out)


def solution(mesh):
    in_specs = (
        P(None, ("kv", "tp")),
        P("kv", "tp", None, None),
        P("kv"),
        P("kv", "tp"),
        P("kv", "tp"),
        P("tp", "kv"),
        P("kv"),
        P("kv", "tp"),
        P("kv", "tp"),
        P("kv", "tp"),
        P("kv", "tp"),
        P("tp"),
        P("tp", "kv"),
        P("kv"),
        P("kv", "tp"),
        P("kv", "tp"),
        P("tp", "kv"),
    )
    out_specs = (P(None, ("kv", "tp")), P("kv", "tp", None, None))
    return jax.shard_map(shards, mesh=mesh, in_specs=in_specs, out_specs=out_specs, check_vma=False)
```

profile of v0, /device:TPU:0, one launch (start us, length us, event | category | flops | bytes accessed | tf_op | source)
XLA Modules:
  0.0 409.7 jit_solution(10858656113238108868)
XLA Ops:
  7.2 15.8 %all_gather.12 = bf16[256,1024]{1,0:T(8,128)(2,1)S(1)} all-gather(bf16[256,128]{1,0:T(8,128)(2,1)} %param.17), channel_id=1, replica_groups=mesh['kv'=4,'tp'=8] {'tp'}, dimensions={1}, use_global_device_ids=true | all-gather | bytes 589824 | tf_op jit(solution)/shard_map/all_gather | solution.py:156
  23.0 2.5 convolution_convert_fusion.2
  27.7 10.1 %psum.43 = bf16[256]{0:T(256)(128)(2,1)S(1)} all-reduce(bf16[256]{0:T(256)(128)(2,1)S(1)} %fusion.3), channel_id=1, replica_groups=mesh['kv'=4,'tp'=8] {'kv'}, use_global_device_ids=true, to_apply=%region_2.0 | all-reduce | flops 256 | bytes 1024 | tf_op jit(solution)/shard_map/psum | solution.py:43
  37.8 48.4 %all-reduce.8.cloned.1.call-done = (bf16[256,1408]{1,0:T(8,128)(2,1)}, bf16[256,1408]{1,0:T(8,128)(2,1)}) async-done(((bf16[256,1408]{1,0:T(8,128)(2,1)}, bf16[256,1408]{1,0:T(8,128)(2,1)}), (bf16[256,1408]{1,0:T(8,128)(2,1)}, bf16[256,1408]{1,0:T(8,128)(2,1)})) %all-reduce.8.cloned.1.call-update) | async-done | bytes 1441808 | tf_op jit(solution)/shard_map/psum | solution.py:42
  86.2 3.5 fusion
  90.8 31.2 %reduce-scatter.22.cloned.1.call-done = bf16[128,256]{1,0:T(8,128)(2,1)} async-done(((bf16[1024,256]{1,0:T(8,128)(2,1)}), bf16[128,256]{1,0:T(8,128)(2,1)}) %reduce-scatter.22.cloned.1.call-update) | async-done | bytes 65552
  123.0 14.0 %all_gather.13 = bf16[256,1024]{1,0:T(8,128)(2,1)S(1)} all-gather(bf16[256,128]{1,0:T(8,128)(2,1)S(1)} %add_convert_fusion.2), channel_id=1, replica_groups=mesh['kv'=4,'tp'=8] {'tp'}, dimensions={1}, use_global_device_ids=true | all-gather | bytes 589824 | tf_op jit(solution)/shard_map/all_gather | solution.py:167
  142.5 2.4 convolution_convert_fusion.5
  145.1 9.9 %all-reduce = bf16[256]{0:T(256)(128)(2,1)S(1)} all-reduce(bf16[256]{0:T(256)(128)(2,1)S(1)} %fusion.5), channel_id=4, replica_groups=mesh['kv'=4,'tp'=8] {'kv'}, use_global_device_ids=true, to_apply=%region_7.8.clone | all-reduce | flops 256 | bytes 1024
  155.2 2.4 convolution_convert_fusion.6
  157.8 4.2 %reduce-scatter.16.cloned.1.call-done = bf16[64,256]{1,0:T(8,128)(2,1)} async-done(((bf16[256,256]{1,0:T(8,128)(2,1)}), bf16[64,256]{1,0:T(8,128)(2,1)}) %reduce-scatter.16.cloned.1.call-update) | async-done | bytes 32784 | tf_op jit(solution)/shard_map/reduce_scatter | solution.py:69
  162.0 26.8 %reduce-scatter.18.cloned.1.call-done = bf16[64,256]{1,0:T(8,128)(2,1)} async-done(((bf16[256,256]{1,0:T(8,128)(2,1)}), bf16[64,256]{1,0:T(8,128)(2,1)}) %reduce-scatter.18.cloned.1.call-update) | async-done | bytes 32784 | tf_op jit(solution)/shard_map/reduce_scatter | solution.py:72
  190.2 26.1 %reduce-scatter.20.cloned.1.call-done = bf16[64,512]{1,0:T(8,128)(2,1)} async-done(((bf16[256,512]{1,0:T(8,128)(2,1)}), bf16[64,512]{1,0:T(8,128)(2,1)}) %reduce-scatter.20.cloned.1.call-update) | async-done | bytes 65552 | tf_op jit(solution)/shard_map/reduce_scatter | solution.py:75
  217.3 5.3 %multiply_add_fusion = f32[64,4,64,128]{3,2,1,0:T(8,128)S(1)} fusion(f32[64,4,64,128]{3,2,1,0:T(8,128)} %param.18, f32[64,4,128]{2,1,0:T(4,128)S(1)} %mul.290, f32[64,4,64]{2,1,0:T(4,128)S(1)} %copy.21, f32[4]{0:T(128)S(1)} %exponential_subtract_fusion), kind=kLoop, calls=%fused_computation | loop fusion | flops 6291456 | bytes 16973840 | tf_op jit(solution)/shard_map/add | solution.py:97
  222.6 7.3 %fusion.30 = f32[64,4,1,128]{3,2,1,0:T(1,128)S(1)} fusion(f32[64,4,64,1]{2,3,1,0:T(1,128)S(1)} %copy.22, f32[64,4,64,128]{3,2,1,0:T(8,128)S(1)} %multiply_add_fusion), kind=kOutput, calls=%fused_computation.64 | convolution fusion | flops 25165824 | bytes 8585216 | tf_op jit(solution)/shard_map/bhk,bhkv->bhv/dot_general | solution.py:100
  230.6 12.7 %reduce-scatter.14.cloned.1.call-done = bf16[64,512]{1,0:T(8,128)(2,1)} async-done(((bf16[256,512]{1,0:T(8,128)(2,1)}), bf16[64,512]{1,0:T(8,128)(2,1)}) %reduce-scatter.14.cloned.1.call-update) | async-done | bytes 65552 | tf_op jit(solution)/shard_map/reduce_scatter | solution.py:78
  244.3 9.3 %all_gather.14 = bf16[256,512]{1,0:T(8,128)(2,1)S(1)} all-gather(bf16[64,512]{1,0:T(8,128)(2,1)S(1)} %fusion.21), channel_id=1, replica_groups=mesh['kv'=4,'tp'=8] {'kv'}, dimensions={0}, use_global_device_ids=true | all-gather | bytes 327680 | tf_op jit(solution)/shard_map/all_gather | solution.py:108
  256.3 31.4 %reduce-scatter.24.cloned.1.call-done = bf16[128,256]{1,0:T(8,128)(2,1)} async-done(((bf16[1024,256]{1,0:T(8,128)(2,1)}), bf16[128,256]{1,0:T(8,128)(2,1)}) %reduce-scatter.24.cloned.1.call-update) | async-done | bytes 65552
  288.7 14.2 %all_gather.15 = bf16[256,1024]{1,0:T(8,128)(2,1)S(1)} all-gather(bf16[256,128]{1,0:T(8,128)(2,1)S(1)} %add_convert_fusion.1), channel_id=1, replica_groups=mesh['kv'=4,'tp'=8] {'tp'}, dimensions={1}, use_global_device_ids=true | all-gather | bytes 589824 | tf_op jit(solution)/shard_map/all_gather | solution.py:167
  302.8 3.7 convolution_convert_fusion
  308.6 10.2 %psum.46 = bf16[256]{0:T(256)(128)(2,1)S(1)} all-reduce(bf16[256]{0:T(256)(128)(2,1)S(1)} %fusion.7), channel_id=1, replica_groups=mesh['kv'=4,'tp'=8] {'kv'}, use_global_device_ids=true, to_apply=%region_16.17 | all-reduce | flops 256 | bytes 1024 | tf_op jit(solution)/shard_map/psum | solution.py:43
  318.9 46.7 %all-reduce.6.cloned.1.call-done = (bf16[256,1408]{1,0:T(8,128)(2,1)}, bf16[256,1408]{1,0:T(8,128)(2,1)}) async-done(((bf16[256,1408]{1,0:T(8,128)(2,1)}, bf16[256,1408]{1,0:T(8,128)(2,1)}), (bf16[256,1408]{1,0:T(8,128)(2,1)}, bf16[256,1408]{1,0:T(8,128)(2,1)})) %all-reduce.6.cloned.1.call-update) | async-done | bytes 1441808 | tf_op jit(solution)/shard_map/psum | solution.py:42
  365.6 3.4 fusion.1
  370.0 31.6 %reduce-scatter.26.cloned.1.call-done = bf16[128,256]{1,0:T(8,128)(2,1)} async-done(((bf16[1024,256]{1,0:T(8,128)(2,1)}), bf16[128,256]{1,0:T(8,128)(2,1)}) %reduce-scatter.26.cloned.1.call-update) | async-done | bytes 65552
  (77 shorter events, 21.9 us)
Async XLA Ops:
  7.2 15.9 %copy-start = (bf16[1024,1408]{1,0:T(8,128)(2,1)S(1)}, bf16[1024,1408]{1,0:T(8,128)(2,1)}, u32[]{:S(2)}) copy-start(bf16[1024,1408]{1,0:T(8,128)(2,1)} %param.21) | copy-start | bytes 8650756
  7.2 18.4 %copy-start.6 = (f32[1024]{0:T(1024)S(1)}, f32[1024]{0:T(1024)}, u32[]{:S(2)}) copy-start(f32[1024]{0:T(1024)} %param.19) | copy-start | bytes 12292
  7.2 79.0 %all-reduce.8.cloned.1.call-start = ((), (), s32[]{:S(2)}) async-start(), calls=%async_computation.15 | async-start | bytes 2883584 | tf_op jit(solution)/shard_map/psum | solution.py:42
  7.2 18.3 %copy-start.4 = (bf16[1024,1408]{1,0:T(8,128)(2,1)S(1)}, bf16[1024,1408]{1,0:T(8,128)(2,1)}, u32[]{:S(2)}) copy-start(bf16[1024,1408]{1,0:T(8,128)(2,1)} %param.20) | copy-start | bytes 8650756
  27.5 94.6 %reduce-scatter.22.cloned.1.call-start = ((), (), s32[]{:S(2)}) async-start(), calls=%async_computation.11 | async-start | bytes 589824
  86.2 36.8 %copy-start.2 = (bf16[256,128]{1,0:T(8,128)(2,1)S(1)}, bf16[256,128]{1,0:T(8,128)(2,1)}, u32[]{:S(2)}) copy-start(bf16[256,128]{1,0:T(8,128)(2,1)} %param.17) | copy-start | bytes 196612
  86.2 50.9 %copy-start.7 = (f32[1024]{0:T(1024)S(1)}, f32[1024]{0:T(1024)}, u32[]{:S(2)}) copy-start(f32[1024]{0:T(1024)} %param.23) | copy-start | bytes 12292
  89.7 49.5 %copy-start.9 = (u32[32]{0:T(128)S(1)}, u32[32]{0:T(128)}, u32[]{:S(2)}) copy-start(u32[32]{0:T(128)} %constant.53) | copy-start | bytes 388
  90.7 71.3 %reduce-scatter.16.cloned.1.call-start = ((), (), s32[]{:S(2)}) async-start(), calls=%async_computation.8 | async-start | bytes 163840 | tf_op jit(solution)/shard_map/reduce_scatter | solution.py:69
  139.1 49.7 %reduce-scatter.18.cloned.1.call-start = ((), (), s32[]{:S(2)}) async-start(), calls=%async_computation.9 | async-start | bytes 163840 | tf_op jit(solution)/shard_map/reduce_scatter | solution.py:72
  142.4 73.9 %reduce-scatter.20.cloned.1.call-start = ((), (), s32[]{:S(2)}) async-start(), calls=%async_computation.10 | async-start | bytes 327680 | tf_op jit(solution)/shard_map/reduce_scatter | solution.py:75
  144.9 98.4 %reduce-scatter.14.cloned.1.call-start = ((), (), s32[]{:S(2)}) async-start(), calls=%async_computation.7 | async-start | bytes 327680 | tf_op jit(solution)/shard_map/reduce_scatter | solution.py:78
  157.6 130.1 %reduce-scatter.24.cloned.1.call-start = ((), (), s32[]{:S(2)}) async-start(), calls=%async_computation.12 | async-start | bytes 589824
  222.6 7.4 %copy-start.1 = (f32[64,4,64,128]{3,2,1,0:T(8,128)}, f32[64,4,64,128]{3,2,1,0:T(8,128)S(1)}, u32[]{:S(2)}) copy-start(f32[64,4,64,128]{3,2,1,0:T(8,128)S(1)} %multiply_add_fusion) | copy-start | bytes 25165828
  222.6 20.7 %copy-start.3 = (f32[512]{0:T(512)S(1)}, f32[512]{0:T(512)}, u32[]{:S(2)}) copy-start(f32[512]{0:T(512)} %param.28) | copy-start | bytes 6148
  230.0 72.8 %copy-start.8 = (f32[1024]{0:T(1024)S(1)}, f32[1024]{0:T(1024)}, u32[]{:S(2)}) copy-start(f32[1024]{0:T(1024)} %param.30) | copy-start | bytes 12292
  256.2 109.3 %all-reduce.6.cloned.1.call-start = ((), (), s32[]{:S(2)}) async-start(), calls=%async_computation.14 | async-start | bytes 2883584 | tf_op jit(solution)/shard_map/psum | solution.py:42
  288.6 17.9 %copy-start.5 = (bf16[1024,1408]{1,0:T(8,128)(2,1)S(1)}, bf16[1024,1408]{1,0:T(8,128)(2,1)}, u32[]{:S(2)}) copy-start(bf16[1024,1408]{1,0:T(8,128)(2,1)} %param.31) | copy-start | bytes 8650756
  308.4 93.2 %reduce-scatter.26.cloned.1.call-start = ((), (), s32[]{:S(2)}) async-start(), calls=%async_computation.13 | async-start | bytes 589824
Sparse Core Ops, SparseCore 0:
  27.6 58.5 all-reduce.7
  90.8 31.1 reduce-scatter.21
  139.2 22.7 reduce-scatter.15
  164.6 24.1 reduce-scatter.17
  192.0 24.3 reduce-scatter.19
  218.9 24.3 reduce-scatter.13
  256.4 31.2 reduce-scatter.23
  308.5 56.9 all-reduce.5
  370.1 31.3 reduce-scatter.25
where the time goes:
time: 411 us; the launch traced here: 410 us
  waiting for transfers between devices  259 us (63%)
  blocking collectives  83.5 us (20%)
  matrix products  34.6 us (8%)
  between operations  14.8 us (4%)
  other arithmetic  10.2 us (2%)
  local copies, waits for them, and re-layouts  6.92 us (2%)
    psum x2, waiting for transfers between devices, channel_mix(): lax.psum(up_part.astype(jnp.bfloat16), 'kv').astype(jnp.float32)  95.1 us
    unnamed x12, waiting for transfers between devices  94.3 us
    all_gather x2, blocking collectives, shards(): widened = lax.all_gather(own_columns, 'tp', axis=1, tiled=True)  28.2 us
    reduce_scatter x1, waiting for transfers between devices, token_mix(): lax.psum_scatter(key_part.astype(jnp.bfloat16), 'kv', scatter_dimension=0...  26.8 us
    reduce_scatter x1, waiting for transfers between devices, token_mix(): lax.psum_scatter(value_part.astype(jnp.bfloat16), 'kv', scatter_dimension...  26.1 us
    psum x2, blocking collectives, channel_mix(): lax.psum(squares.astype(jnp.bfloat16), 'kv').astype(jnp.float32)  20.3 us
    all_gather x1, blocking collectives, shards(): widened = lax.all_gather(tokens, 'tp', axis=1, tiled=True)  15.8 us
    reduce_scatter x1, waiting for transfers between devices, token_mix(): lax.psum_scatter(gate_part.astype(jnp.bfloat16), 'kv', scatter_dimension=...  12.7 us
  transfers between devices with their start and end apart: 9, of which 9 were waited for; matrix products, arithmetic and copies ran while one was open for 6% of the time, Pallas kernels for 0%

commit v1 on v0

--- a/solution.py
+++ b/solution.py
@@ -164,7 +164,7 @@
         ).astype(jnp.float32)
         own_columns = (own_columns.astype(jnp.float32) + own_piece).astype(jnp.bfloat16)
         if section_index < 2:
-            widened = lax.all_gather(own_columns, "tp", axis=1, tiled=True)
+            widened = jnp.concatenate(lax.all_gather(own_columns, "tp"), axis=1)
     return (own_columns, state_out)
 
 

time: 411 us -> 422 us (1.027)
  local copies, waits for them, and re-layouts: 6.92 us -> 12.9 us
  other arithmetic: 10.2 us -> 15.3 us
    reduce_scatter x1, waiting for transfers between devices: 26.8 us -> 3.41 us  [token_mix(): lax.psum_scatter(key_part.astype(jnp.bfloat16), 'kv', scatter_dimension=0...]
    reduce_scatter x1, waiting for transfers between devices: 4.2 us -> 26.8 us  [token_mix(): lax.psum_scatter(query_part.astype(jnp.bfloat16), 'kv', scatter_dimension...]
    convert_element_type x0 -> x2, local copies, waits for them, and re-layouts: none -> 5.16 us  [the longest x1 2.59 us: channel_mix(): widened_f = widened.astype(jnp.float32)]
    convert_element_type x0 -> x4, other arithmetic: none -> 5.1 us  [the longest x1 1.57 us: channel_mix(): scaled = (widened_f * gain).astype(jnp.bfloat16)]
where the time goes in v1:
time: 422 us
  waiting for transfers between devices  258 us (61%)
  blocking collectives  84.9 us (20%)
  matrix products  35.2 us (8%)
  other arithmetic  15.3 us (4%)
  between operations  14.8 us (4%)
  local copies, waits for them, and re-layouts  12.9 us (3%)
    psum x2, waiting for transfers between devices, channel_mix(): lax.psum(up_part.astype(jnp.bfloat16), 'kv').astype(jnp.float32)  94.9 us
    unnamed x12, waiting for transfers between devices  94.5 us
    all_gather x2, blocking collectives, shards(): widened = jnp.concatenate(lax.all_gather(own_columns, 'tp'), axis=1)  30.1 us
    reduce_scatter x1, waiting for transfers between devices, token_mix(): lax.psum_scatter(query_part.astype(jnp.bfloat16), 'kv', scatter_dimension...  26.8 us
    reduce_scatter x1, waiting for transfers between devices, token_mix(): lax.psum_scatter(value_part.astype(jnp.bfloat16), 'kv', scatter_dimension...  25.6 us
    psum x2, blocking collectives, channel_mix(): lax.psum(squares.astype(jnp.bfloat16), 'kv').astype(jnp.float32)  20.1 us
    all_gather x1, blocking collectives, shards(): widened = lax.all_gather(tokens, 'tp', axis=1, tiled=True)  15.8 us
    reduce_scatter x1, waiting for transfers between devices, token_mix(): lax.psum_scatter(gate_part.astype(jnp.bfloat16), 'kv', scatter_dimension=...  12.7 us
  transfers between devices with their start and end apart: 9, of which 9 were waited for; matrix products, arithmetic and copies ran while one was open for 6% of the time, Pallas kernels for 0%

profile of v1, /device:TPU:0, one launch (start us, length us, event | category | flops | bytes accessed | tf_op | source)
XLA Modules:
  0.0 421.6 jit_solution(11288777733232759057)
XLA Ops:
  7.2 15.8 %all_gather.18 = bf16[256,1024]{1,0:T(8,128)(2,1)S(1)} all-gather(bf16[256,128]{1,0:T(8,128)(2,1)} %param.17), channel_id=1, replica_groups=mesh['kv'=4,'tp'=8] {'tp'}, dimensions={1}, use_global_device_ids=true | all-gather | bytes 589824 | tf_op jit(solution)/shard_map/all_gather | solution.py:156
  27.7 10.1 %psum.43 = bf16[256]{0:T(256)(128)(2,1)S(1)} all-reduce(bf16[256]{0:T(256)(128)(2,1)S(1)} %fusion.3), channel_id=1, replica_groups=mesh['kv'=4,'tp'=8] {'kv'}, use_global_device_ids=true, to_apply=%region_2.0 | all-reduce | flops 256 | bytes 1024 | tf_op jit(solution)/shard_map/psum | solution.py:43
  37.8 48.4 %all-reduce.8.cloned.1.call-done = (bf16[256,1408]{1,0:T(8,128)(2,1)}, bf16[256,1408]{1,0:T(8,128)(2,1)}) async-done(((bf16[256,1408]{1,0:T(8,128)(2,1)}, bf16[256,1408]{1,0:T(8,128)(2,1)}), (bf16[256,1408]{1,0:T(8,128)(2,1)}, bf16[256,1408]{1,0:T(8,128)(2,1)})) %all-reduce.8.cloned.1.call-update) | async-done | bytes 1441808 | tf_op jit(solution)/shard_map/psum | solution.py:42
  86.2 3.5 fusion
  90.8 31.5 %reduce-scatter.22.cloned.1.call-done = bf16[128,256]{1,0:T(8,128)(2,1)} async-done(((bf16[1024,256]{1,0:T(8,128)(2,1)}), bf16[128,256]{1,0:T(8,128)(2,1)}) %reduce-scatter.22.cloned.1.call-update) | async-done | bytes 65552
  123.3 14.9 %all-gather = bf16[2048,128]{1,0:T(8,128)(2,1)S(1)} all-gather(bf16[256,128]{1,0:T(8,128)(2,1)S(1)} %add_convert_fusion.2), channel_id=2, replica_groups=mesh['kv'=4,'tp'=8] {'tp'}, dimensions={0}, use_global_device_ids=true | all-gather | bytes 589824 | tf_op jit(solution)/shard_map/all_gather | solution.py:167
  139.2 2.6 copy.23
  149.7 2.6 convolution_convert_fusion.5
  152.5 9.7 %all-reduce = bf16[256]{0:T(256)(128)(2,1)S(1)} all-reduce(bf16[256]{0:T(256)(128)(2,1)S(1)} %fusion.4), channel_id=6, replica_groups=mesh['kv'=4,'tp'=8] {'kv'}, use_global_device_ids=true, to_apply=%region_7.8.clone | all-reduce | flops 256 | bytes 1024
  165.1 3.4 reduce-scatter.18.cloned.1.call-done
  168.5 26.8 %reduce-scatter.16.cloned.1.call-done = bf16[64,256]{1,0:T(8,128)(2,1)} async-done(((bf16[256,256]{1,0:T(8,128)(2,1)}), bf16[64,256]{1,0:T(8,128)(2,1)}) %reduce-scatter.16.cloned.1.call-update) | async-done | bytes 32784 | tf_op jit(solution)/shard_map/reduce_scatter | solution.py:69
  196.7 25.6 %reduce-scatter.20.cloned.1.call-done = bf16[64,512]{1,0:T(8,128)(2,1)} async-done(((bf16[256,512]{1,0:T(8,128)(2,1)}), bf16[64,512]{1,0:T(8,128)(2,1)}) %reduce-scatter.20.cloned.1.call-update) | async-done | bytes 65552 | tf_op jit(solution)/shard_map/reduce_scatter | solution.py:75
  223.2 5.3 %multiply_add_fusion = f32[64,4,64,128]{3,2,1,0:T(8,128)S(1)} fusion(f32[64,4,64,128]{3,2,1,0:T(8,128)} %param.18, f32[64,4,128]{2,1,0:T(4,128)S(1)} %mul.294, f32[64,4,64]{2,1,0:T(4,128)S(1)} %copy.26, f32[4]{0:T(128)S(1)} %exponential_subtract_fusion), kind=kLoop, calls=%fused_computation | loop fusion | flops 6291456 | bytes 16973840 | tf_op jit(solution)/shard_map/add | solution.py:97
  228.6 7.3 %fusion.24 = f32[64,4,1,128]{3,2,1,0:T(1,128)S(1)} fusion(f32[64,4,64,1]{2,3,1,0:T(1,128)S(1)} %copy.28, f32[64,4,64,128]{3,2,1,0:T(8,128)S(1)} %multiply_add_fusion), kind=kOutput, calls=%fused_computation.66 | convolution fusion | flops 25165824 | bytes 8585216 | tf_op jit(solution)/shard_map/bhk,bhkv->bhv/dot_general | solution.py:100
  236.5 12.7 %reduce-scatter.14.cloned.1.call-done = bf16[64,512]{1,0:T(8,128)(2,1)} async-done(((bf16[256,512]{1,0:T(8,128)(2,1)}), bf16[64,512]{1,0:T(8,128)(2,1)}) %reduce-scatter.14.cloned.1.call-update) | async-done | bytes 65552 | tf_op jit(solution)/shard_map/reduce_scatter | solution.py:78
  250.2 9.3 %all_gather.21 = bf16[256,512]{1,0:T(8,128)(2,1)S(1)} all-gather(bf16[64,512]{1,0:T(8,128)(2,1)S(1)} %fusion.15), channel_id=1, replica_groups=mesh['kv'=4,'tp'=8] {'kv'}, dimensions={0}, use_global_device_ids=true | all-gather | bytes 327680 | tf_op jit(solution)/shard_map/all_gather | solution.py:108
  262.2 31.5 %reduce-scatter.24.cloned.1.call-done = bf16[128,256]{1,0:T(8,128)(2,1)} async-done(((bf16[1024,256]{1,0:T(8,128)(2,1)}), bf16[128,256]{1,0:T(8,128)(2,1)}) %reduce-scatter.24.cloned.1.call-update) | async-done | bytes 65552
  294.7 15.2 %all-gather.1 = bf16[2048,128]{1,0:T(8,128)(2,1)S(1)} all-gather(bf16[256,128]{1,0:T(8,128)(2,1)S(1)} %add_convert_fusion.1), channel_id=3, replica_groups=mesh['kv'=4,'tp'=8] {'tp'}, dimensions={0}, use_global_device_ids=true | all-gather | bytes 589824 | tf_op jit(solution)/shard_map/all_gather | solution.py:167
  310.9 2.6 copy.27
  315.1 3.7 convolution_convert_fusion
  321.0 10.0 %psum.46 = bf16[256]{0:T(256)(128)(2,1)S(1)} all-reduce(bf16[256]{0:T(256)(128)(2,1)S(1)} %fusion.5), channel_id=1, replica_groups=mesh['kv'=4,'tp'=8] {'kv'}, use_global_device_ids=true, to_apply=%region_16.17 | all-reduce | flops 256 | bytes 1024 | tf_op jit(solution)/shard_map/psum | solution.py:43
  331.0 46.5 %all-reduce.6.cloned.1.call-done = (bf16[256,1408]{1,0:T(8,128)(2,1)}, bf16[256,1408]{1,0:T(8,128)(2,1)}) async-done(((bf16[256,1408]{1,0:T(8,128)(2,1)}, bf16[256,1408]{1,0:T(8,128)(2,1)}), (bf16[256,1408]{1,0:T(8,128)(2,1)}, bf16[256,1408]{1,0:T(8,128)(2,1)})) %all-reduce.6.cloned.1.call-update) | async-done | bytes 1441808 | tf_op jit(solution)/shard_map/psum | solution.py:42
  377.5 3.4 fusion.1
  382.0 31.5 %reduce-scatter.26.cloned.1.call-done = bf16[128,256]{1,0:T(8,128)(2,1)} async-done(((bf16[1024,256]{1,0:T(8,128)(2,1)}), bf16[128,256]{1,0:T(8,128)(2,1)}) %reduce-scatter.26.cloned.1.call-update) | async-done | bytes 65552
  (85 shorter events, 33.1 us)
Async XLA Ops:
  7.2 15.9 %copy-start = (bf16[1024,1408]{1,0:T(8,128)(2,1)S(1)}, bf16[1024,1408]{1,0:T(8,128)(2,1)}, u32[]{:S(2)}) copy-start(bf16[1024,1408]{1,0:T(8,128)(2,1)} %param.21) | copy-start | bytes 8650756
  7.2 18.4 %copy-start.9 = (f32[1024]{0:T(1024)S(1)}, f32[1024]{0:T(1024)}, u32[]{:S(2)}) copy-start(f32[1024]{0:T(1024)} %param.19) | copy-start | bytes 12292
  7.2 79.0 %all-reduce.8.cloned.1.call-start = ((), (), s32[]{:S(2)}) async-start(), calls=%async_computation.15 | async-start | bytes 2883584 | tf_op jit(solution)/shard_map/psum | solution.py:42
  7.2 18.3 %copy-start.7 = (bf16[1024,1408]{1,0:T(8,128)(2,1)S(1)}, bf16[1024,1408]{1,0:T(8,128)(2,1)}, u32[]{:S(2)}) copy-start(bf16[1024,1408]{1,0:T(8,128)(2,1)} %param.20) | copy-start | bytes 8650756
  27.5 94.8 %reduce-scatter.22.cloned.1.call-start = ((), (), s32[]{:S(2)}) async-start(), calls=%async_computation.11 | async-start | bytes 589824
  86.2 37.0 %copy-start.3 = (bf16[256,128]{1,0:T(8,128)(2,1)S(1)}, bf16[256,128]{1,0:T(8,128)(2,1)}, u32[]{:S(2)}) copy-start(bf16[256,128]{1,0:T(8,128)(2,1)} %param.17) | copy-start | bytes 196612
  89.7 52.2 %copy-start.4 = (f32[1024]{0:T(1024)S(1)}, f32[1024]{0:T(1024)}, u32[]{:S(2)}) copy-start(f32[1024]{0:T(1024)} %param.23) | copy-start | bytes 12292
  90.7 77.8 %reduce-scatter.18.cloned.1.call-start = ((), (), s32[]{:S(2)}) async-start(), calls=%async_computation.9 | async-start | bytes 163840 | tf_op jit(solution)/shard_map/reduce_scatter | solution.py:72
  139.2 6.9 %copy-start.10 = (u32[32]{0:T(128)S(1)}, u32[32]{0:T(128)}, u32[]{:S(2)}) copy-start(u32[32]{0:T(128)} %constant.53) | copy-start | bytes 388
  143.2 0.8 copy-start.2
  146.1 49.2 %reduce-scatter.16.cloned.1.call-start = ((), (), s32[]{:S(2)}) async-start(), calls=%async_computation.8 | async-start | bytes 163840 | tf_op jit(solution)/shard_map/reduce_scatter | solution.py:69
  149.6 72.6 %reduce-scatter.20.cloned.1.call-start = ((), (), s32[]{:S(2)}) async-start(), calls=%async_computation.10 | async-start | bytes 327680 | tf_op jit(solution)/shard_map/reduce_scatter | solution.py:75
  152.3 97.0 %reduce-scatter.14.cloned.1.call-start = ((), (), s32[]{:S(2)}) async-start(), calls=%async_computation.7 | async-start | bytes 327680 | tf_op jit(solution)/shard_map/reduce_scatter | solution.py:78
  164.8 128.9 %reduce-scatter.24.cloned.1.call-start = ((), (), s32[]{:S(2)}) async-start(), calls=%async_computation.12 | async-start | bytes 589824
  228.5 7.4 %copy-start.1 = (f32[64,4,64,128]{3,2,1,0:T(8,128)}, f32[64,4,64,128]{3,2,1,0:T(8,128)S(1)}, u32[]{:S(2)}) copy-start(f32[64,4,64,128]{3,2,1,0:T(8,128)S(1)} %multiply_add_fusion) | copy-start | bytes 25165828
  228.6 20.7 %copy-start.6 = (f32[512]{0:T(512)S(1)}, f32[512]{0:T(512)}, u32[]{:S(2)}) copy-start(f32[512]{0:T(512)} %param.28) | copy-start | bytes 6148
  261.1 52.4 %copy-start.5 = (f32[1024]{0:T(1024)S(1)}, f32[1024]{0:T(1024)}, u32[]{:S(2)}) copy-start(f32[1024]{0:T(1024)} %param.30) | copy-start | bytes 12292
  262.2 115.3 %all-reduce.6.cloned.1.call-start = ((), (), s32[]{:S(2)}) async-start(), calls=%async_computation.14 | async-start | bytes 2883584 | tf_op jit(solution)/shard_map/psum | solution.py:42
  313.5 5.3 %copy-start.8 = (bf16[1024,1408]{1,0:T(8,128)(2,1)S(1)}, bf16[1024,1408]{1,0:T(8,128)(2,1)}, u32[]{:S(2)}) copy-start(bf16[1024,1408]{1,0:T(8,128)(2,1)} %param.31) | copy-start | bytes 8650756
  320.7 92.7 %reduce-scatter.26.cloned.1.call-start = ((), (), s32[]{:S(2)}) async-start(), calls=%async_computation.13 | async-start | bytes 589824
Sparse Core Ops, SparseCore 0:
  27.6 58.5 all-reduce.7
  90.8 31.3 reduce-scatter.21
  146.2 22.1 reduce-scatter.17
  171.1 24.1 reduce-scatter.15
  197.9 24.3 reduce-scatter.19
  224.9 24.3 reduce-scatter.13
  262.3 31.3 reduce-scatter.23
  320.8 56.5 all-reduce.5
  382.1 31.2 reduce-scatter.25
